TPU v7x, 256 devices: a whole 4x4x8 slice. The times are simulated.
256 devices in a mesh: ep: 64 (over z, x, core), tp: 4 (over y).
Axes of the slice: x: 4, y: 4, z: 8, core: 2. Of those that a mesh axis runs over, the one named last changes fastest.
Arguments:
- conv_value: bfloat16 [65536, 1024], P('ep', 'tp'), may hold values from -600 to 600
- conv_gate: bfloat16 [65536, 1024], P('ep', 'tp'), may hold values from -8 to 8
- depth_weight: float32 [31, 1024], replicated, may hold values from -1 to 1
- norm_gain: float32 [1024], replicated, may hold values from 0.1 to 1.9
- norm_shift: float32 [1024], replicated, may hold values from -3 to 3
- conv_out_weight: bfloat16 [1024, 2048], P('tp'), may hold values from -0.1875 to 0.1875
- moe_input: bfloat16 [98304, 2048], P(('ep', 'tp')), may hold values from -6 to 6
- moe_gain: float32 [2048], replicated, may hold values from 0.1 to 1.9
- route_experts: int32 [98304, 2], P(('ep', 'tp')), may hold values from 0 to 63, as said below
- route_scores: float32 [98304, 2], P(('ep', 'tp')), may hold values from -8 to 8
- expert_gate: bfloat16 [64, 2048, 512], P('ep'), may hold values from -0.125 to 0.125
- expert_up: bfloat16 [64, 2048, 512], P('ep'), may hold values from -0.125 to 0.125
- expert_down: bfloat16 [64, 512, 2048], P('ep'), may hold values from -1 to 1
Outputs:
- conv_out: bfloat16 [65536, 2048], P(('ep', 'tp'))
- moe_out: bfloat16 [98304, 2048], P(('ep', 'tp'))
Inputs may be any that keep to these rules, and one draw needn't show every extreme that they name: `route_experts`: each row names two different experts that lie in one group of 16 consecutive experts.
All inputs are finite; a program needn't handle non-finite values.
Results may differ from a plain program's by a relative error of at most 0.009.
Values may be sent and summed in bfloat16 or wider, within the bound.
No kernel may reach another device: no remote copies, remote signals or barrier semaphores. Data moves between devices by JAX's collectives and lax.ppermute only.
A program may use at most 128 MiB of HBM per device.

v0:
```python
import jax
import jax.numpy as jnp
from jax import lax
from jax.sharding import PartitionSpec as P

CONV = 1024
TOP = 2


def passed_along(x, axis, by):
    peers = lax.axis_size(axis)
    pairs = [(i, i + by) for i in range(peers) if 0 <= i + by < peers]
    return lax.ppermute(x, axis, pairs)


def conv_half(conv_value, conv_gate, depth_weight, norm_gain, norm_shift, conv_out_weight):
    channels = conv_value.shape[1]
    length = conv_value.shape[0]
    first_col = lax.axis_index("tp") * channels
    taps = lax.dynamic_slice_in_dim(depth_weight, first_col, channels, 1)
    gains = lax.dynamic_slice_in_dim(norm_gain, first_col, channels, 0)
    shifts = lax.dynamic_slice_in_dim(norm_shift, first_col, channels, 0)
    gated = (conv_value.astype(jnp.float32) * jax.nn.sigmoid(conv_gate.astype(jnp.float32))).astype(
        jnp.bfloat16
    )
    reach = taps.shape[0] - 1
    earlier = passed_along(gated[length - reach :], "ep", 1)
    padded = jnp.concatenate([earlier, gated], 0).astype(jnp.float32)
    filtered = taps[0] * padded[0:length]
    for offset in range(1, reach + 1):
        filtered = filtered + taps[offset] * padded[offset : offset + length]
    sums, squares = lax.psum(
        (jnp.sum(filtered, axis=1), jnp.sum(filtered * filtered, axis=1)), "tp"
    )
    center = (sums / CONV)[:, None]
    spread = (squares / CONV)[:, None] - center * center
    normed = (filtered - center) * lax.rsqrt(spread + 1e-05) * gains + shifts
    activated = jax.nn.silu(normed).astype(jnp.bfloat16)
    partial_value = jnp.dot(activated, conv_out_weight, preferred_element_type=jnp.float32)
    return lax.psum_scatter(
        partial_value.astype(jnp.bfloat16).astype(jnp.float32).astype(jnp.bfloat16),
        "tp",
        scatter_dimension=0,
        tiled=True,
    )


def moe_half(moe_input, moe_gain, route_experts, route_scores, expert_gate, expert_up, expert_down):
    rows = moe_input.shape[0]
    model_width = moe_input.shape[1]
    experts_all = lax.axis_size("ep")
    capacity = 2 * (3 * TOP * rows // (4 * experts_all))
    widened = moe_input.astype(jnp.float32)
    normal_in = (
        widened * lax.rsqrt(jnp.mean(widened * widened, axis=-1, keepdims=True) + 1e-06) * moe_gain
    ).astype(jnp.bfloat16)
    chosen = route_experts.reshape(-1)
    onehot = (chosen[:, None] == jnp.arange(experts_all, dtype=jnp.int32)[None, :]).astype(
        jnp.int32
    )
    slot_rank = jnp.sum(jnp.cumsum(onehot, axis=0) * onehot, axis=-1) - 1
    slot_index = jnp.where(
        slot_rank < capacity, chosen * capacity + slot_rank, experts_all * capacity
    )
    source_row = jnp.arange(rows * TOP, dtype=jnp.int32) // TOP
    slot_token = (
        jnp.full((experts_all * capacity,), rows, jnp.int32)
        .at[slot_index]
        .set(source_row, mode="drop")
    )
    padded_in = jnp.concatenate([normal_in, jnp.zeros((1, model_width), jnp.bfloat16)], 0)
    send_buffer = padded_in[slot_token].reshape(experts_all, capacity, model_width)
    arrived = lax.all_to_all(send_buffer, "ep", split_axis=0, concat_axis=0, tiled=True)
    flat_rows = arrived.reshape(-1, model_width)
    gate_act = jnp.dot(flat_rows, expert_gate[0], preferred_element_type=jnp.float32)
    up_act = jnp.dot(flat_rows, expert_up[0], preferred_element_type=jnp.float32)
    inner = (jax.nn.silu(gate_act) * up_act).astype(jnp.bfloat16)
    result = jnp.dot(inner, expert_down[0], preferred_element_type=jnp.float32).astype(jnp.bfloat16)
    returned = lax.all_to_all(
        result.reshape(arrived.shape), "ep", split_axis=0, concat_axis=0, tiled=True
    )
    returned_flat = jnp.concatenate(
        [
            returned.reshape(experts_all * capacity, model_width),
            jnp.zeros((1, model_width), jnp.bfloat16),
        ],
        0,
    )
    picked = returned_flat[slot_index].reshape(rows, TOP, model_width)
    group_gate = jax.nn.sigmoid(route_scores[:, 0])
    first_weight = (group_gate * jax.nn.sigmoid(route_scores[:, 1]))[:, None]
    second_weight = (group_gate * jax.nn.sigmoid(-route_scores[:, 1]))[:, None]
    combined = first_weight * picked[:, 0].astype(jnp.float32) + second_weight * picked[
        :, 1
    ].astype(jnp.float32)
    return combined.astype(jnp.bfloat16)


def on_device(
    conv_value,
    conv_gate,
    depth_weight,
    norm_gain,
    norm_shift,
    conv_out_weight,
    moe_input,
    moe_gain,
    route_experts,
    route_scores,
    expert_gate,
    expert_up,
    expert_down,
):
    conv_out = conv_half(
        conv_value, conv_gate, depth_weight, norm_gain, norm_shift, conv_out_weight
    )
    moe_out = moe_half(
        moe_input, moe_gain, route_experts, route_scores, expert_gate, expert_up, expert_down
    )
    return (conv_out, moe_out)


def solution(mesh):
    in_specs = (
        P("ep", "tp"),
        P("ep", "tp"),
        P(),
        P(),
        P(),
        P("tp", None),
        P(("ep", "tp"), None),
        P(),
        P(("ep", "tp"), None),
        P(("ep", "tp"), None),
        P("ep", None, None),
        P("ep", None, None),
        P("ep", None, None),
    )
    out_specs = (P(("ep", "tp"), None), P(("ep", "tp"), None))
    return jax.shard_map(
        on_device, mesh=mesh, in_specs=in_specs, out_specs=out_specs, check_vma=False
    )
```

profile of v0, /device:TPU:96, one launch (start us, length us, event | category | flops | bytes accessed | tf_op | source)
XLA Modules:
  0.0 418.5 jit_solution(11810844819671577286)
XLA Ops:
  9.2 1.8 reduce-window.6
  11.8 3.4 scatter_custom_fusion
  15.2 1.8 fusion
  17.0 1.8 fusion.2
  20.1 12.3 %gather_fusion = bf16[1152,2048]{1,0:T(8,128)(2,1)} fusion(bf16[385,2048]{1,0:T(8,128)(2,1)} %concatenate.10, s32[2048]{0:T(1024)S(1)} %pad_clamp_fusion), kind=kCustom, calls=%fused_computation | custom fusion | bytes 9441792 | tf_op jit(solution)/shard_map/gather | solution.py:72
  32.4 7.6 %reshape.112 = bf16[64,18,2048]{2,1,0:T(8,128)(2,1)} reshape(bf16[1152,2048]{1,0:T(8,128)(2,1)} %gather_fusion) | data formatting | bytes 9437184 | tf_op jit(solution)/shard_map/reshape | solution.py:72
  40.0 11.0 %all-to-all-start = ((bf16[64,18,2048]{2,1,0:T(8,128)(2,1)}), bf16[64,18,2048]{2,1,0:T(8,128)(2,1)}, u32[]{:S(2)}, u32[]{:S(2)}) async-start(bf16[64,18,2048]{2,1,0:T(8,128)(2,1)} %reshape.112), calls=%async_computation.1 | async-start | bytes 12582912 | tf_op jit(solution)/shard_map/all_to_all | solution.py:73
  52.4 2.2 collective-permute-start
  55.9 133.4 %all-to-all-done = bf16[64,18,2048]{2,1,0:T(8,128)(2,1)} async-done(((bf16[64,18,2048]{2,1,0:T(8,128)(2,1)}), bf16[64,18,2048]{2,1,0:T(8,128)(2,1)}, u32[]{:S(2)}, u32[]{:S(2)}) %all-to-all-start) | async-done | bytes 4718624 | tf_op jit(solution)/shard_map/all_to_all | solution.py:73
  189.3 7.8 %reshape.113 = bf16[1152,2048]{1,0:T(8,128)(2,1)} reshape(bf16[64,18,2048]{2,1,0:T(8,128)(2,1)} %all-to-all-done) | data formatting | bytes 9437184 | tf_op jit(solution)/shard_map/reshape | solution.py:74
  197.0 7.1 %fusion.8 = f32[1152,512]{1,0:T(8,128)} fusion(bf16[1152,2048]{1,0:T(8,128)(2,1)} %reshape.113, bf16[1,2048,512]{2,1,0:T(8,128)(2,1)} %param.23), kind=kOutput, calls=%fused_computation.18 | convolution fusion | flops 2415919104 | bytes 9175040 | tf_op jit(solution)/shard_map/dot_general | solution.py:75
  204.2 11.0 %convolution_convert_fusion = bf16[1152,2048]{1,0:T(8,128)(2,1)} fusion(bf16[1,512,2048]{2,1,0:T(8,128)(2,1)S(1)} %copy-done, bf16[1152,2048]{1,0:T(8,128)(2,1)} %reshape.113, f32[1152,512]{1,0:T(8,128)} %fusion.8, bf16[1,2048,512]{2,1,0:T(8,128)(2,1)} %param.24), kind=kOutput, calls=%fused_computation.3 | convolution fusion | flops 4837736448 | bytes 15990784 | tf_op jit(solution)/shard_map/dot_general | solution.py:78
  215.2 7.6 %reshape.114 = bf16[64,18,2048]{2,1,0:T(8,128)(2,1)} reshape(bf16[1152,2048]{1,0:T(8,128)(2,1)} %convolution_convert_fusion) | data formatting | bytes 9437184 | tf_op jit(solution)/shard_map/reshape | solution.py:80
  222.7 8.7 %all-to-all-start.1 = ((bf16[64,18,2048]{2,1,0:T(8,128)(2,1)}), bf16[64,18,2048]{2,1,0:T(8,128)(2,1)}, u32[]{:S(2)}, u32[]{:S(2)}) async-start(bf16[64,18,2048]{2,1,0:T(8,128)(2,1)} %reshape.114), calls=%async_computation.2 | async-start | bytes 12582912 | tf_op jit(solution)/shard_map/all_to_all | solution.py:79
  234.3 4.5 %fusion.61 = (f32[1024]{0:T(1024)S(1)}, f32[1024]{0:T(1024)S(1)}, f32[1024,256]{1,0:T(8,128)S(1)}) fusion(f32[1054,256]{1,0:T(8,128)S(1)} %maximum_convert_fusion, f32[256]{0:T(256)S(1)} %bitcast.102, f32[256]{0:T(256)S(1)} %bitcast.73, f32[256]{0:T(256)S(1)} %bitcast.74, f32[256]{0:T(256)S(1)} %bitcast.75, f32[256]{0:T(256)S(1)} %bitcast.76, ...), kind=kLoop, calls=%fused_computation.130 | loop fusion | flops 16775168 | bytes 33594368 | tf_op jit(solution)/shard_map/reduce_sum | solution.py:33
  238.8 11.1 %all-reduce.2 = (f32[1024]{0:T(1024)S(1)}, f32[1024]{0:T(1024)S(1)}) all-reduce(f32[1024]{0:T(1024)S(1)} %get-tuple-element.3, f32[1024]{0:T(1024)S(1)} %get-tuple-element.2), channel_id=1, replica_groups=mesh['ep'=64,'tp'=4] {'tp'}, use_global_device_ids=true, to_apply=%region_3.0 | all-reduce | flops 2048 | bytes 16384 | tf_op jit(solution)/shard_map/psum | solution.py:32
  249.9 4.6 %convolution_convert_fusion.1 = bf16[1024,2048]{1,0:T(8,128)(2,1)} fusion(bf16[256,2048]{1,0:T(8,128)(2,1)} %param.18, f32[1024,256]{1,0:T(8,128)S(1)} %get-tuple-element.10, f32[256]{0:T(256)S(1)} %dynamic_slice.11, f32[256]{0:T(256)S(1)} %dynamic_slice.10, f32[1024]{0:T(1024)S(1)} %get-tuple-element.45, f32[1024]{0:T(1024)S(1)} %get-tuple-element.44), kind=kOutput, calls=%fused_computation.6 | convolution fusion | flops 1078198272 | bytes 6301696 | tf_op jit(solution)/shard_map/dot_general | solution.py:39
  255.2 114.5 %all-to-all-done.1 = bf16[64,18,2048]{2,1,0:T(8,128)(2,1)} async-done(((bf16[64,18,2048]{2,1,0:T(8,128)(2,1)}), bf16[64,18,2048]{2,1,0:T(8,128)(2,1)}, u32[]{:S(2)}, u32[]{:S(2)}) %all-to-all-start.1) | async-done | bytes 4718624 | tf_op jit(solution)/shard_map/all_to_all | solution.py:79
  369.7 7.8 %reshape.115 = bf16[1152,2048]{1,0:T(8,128)(2,1)} reshape(bf16[64,18,2048]{2,1,0:T(8,128)(2,1)} %all-to-all-done.1) | data formatting | bytes 9437184 | tf_op jit(solution)/shard_map/reshape | solution.py:84
  377.5 5.2 %concatenate.11 = bf16[1153,2048]{1,0:T(8,128)(2,1)} pad(bf16[1152,2048]{1,0:T(8,128)(2,1)} %reshape.115, bf16[]{:T(256)} %constant.58.clone.1), padding=0_1x0_0 | pad | bytes 9441282 | tf_op jit(solution)/shard_map/concatenate | solution.py:82
  382.7 10.0 %gather_fusion.1 = bf16[768,2048]{1,0:T(8,128)(2,1)} fusion(bf16[1153,2048]{1,0:T(8,128)(2,1)} %concatenate.11, s32[1024]{0:T(1024)S(1)} %pad_clamp_fusion.1), kind=kCustom, calls=%fused_computation.1 | custom fusion | bytes 6294528 | tf_op jit(solution)/shard_map/gather | solution.py:89
  392.7 6.0 %reshape.116 = bf16[384,2,2048]{2,1,0:T(2,128)(2,1)} reshape(bf16[768,2048]{1,0:T(8,128)(2,1)} %gather_fusion.1) | data formatting | bytes 6291456 | tf_op jit(solution)/shard_map/reshape | solution.py:89
  398.8 7.9 %fusion.63 = (bf16[384,1,2048]{2,1,0:T(2,128)(2,1)S(1)}, bf16[384,1,2048]{2,1,0:T(2,128)(2,1)S(1)}) fusion(bf16[384,2,2048]{2,1,0:T(2,128)(2,1)} %reshape.116), kind=kLoop, calls=%fused_computation.131 | loop fusion | bytes 6291456 | tf_op jit(solution)/shard_map/slice | solution.py:93
  406.7 4.9 %fusion.4 = bf16[384,2048]{1,0:T(8,128)(2,1)} fusion(bf16[384,1,2048]{2,1,0:T(2,128)(2,1)S(1)} %get-tuple-element.12, bf16[384,1,2048]{2,1,0:T(2,128)(2,1)S(1)} %get-tuple-element.11, f32[384]{0:T(512)S(1)} %get-tuple-element.5, f32[384]{0:T(512)S(1)} %get-tuple-element.4), kind=kLoop, calls=%fused_computation.13 | loop fusion | flops 4718592 | bytes 4721664 | tf_op jit(solution)/shard_map/convert_element_type | solution.py:96
  (41 shorter events, 10.1 us)
Async XLA Ops:
  7.2 197.0 %copy-start = (bf16[1,512,2048]{2,1,0:T(8,128)(2,1)S(1)}, bf16[1,512,2048]{2,1,0:T(8,128)(2,1)}, u32[]{:S(2)}) copy-start(bf16[1,512,2048]{2,1,0:T(8,128)(2,1)} %param.25) | copy-start | bytes 6291460
  7.2 9.8 %copy-start.3 = (f32[2048]{0:T(1024)S(1)}, f32[2048]{0:T(1024)}, u32[]{:S(2)}) copy-start(f32[2048]{0:T(1024)} %param.20) | copy-start | bytes 24580
  40.0 11.0 %copy-start.2 = (bf16[1024,256]{1,0:T(8,128)(2,1)S(1)}, bf16[1024,256]{1,0:T(8,128)(2,1)}, u32[]{:S(2)}) copy-start(bf16[1024,256]{1,0:T(8,128)(2,1)} %param.14) | copy-start | bytes 1572868
  40.0 149.3 %all-to-all-start = ((bf16[64,18,2048]{2,1,0:T(8,128)(2,1)}), bf16[64,18,2048]{2,1,0:T(8,128)(2,1)}, u32[]{:S(2)}, u32[]{:S(2)}) async-start(bf16[64,18,2048]{2,1,0:T(8,128)(2,1)} %reshape.112), calls=%async_computation.1 | async-start | bytes 12582912 | tf_op jit(solution)/shard_map/all_to_all | solution.py:73
  52.4 181.7 %collective-permute-start = (bf16[30,256]{1,0:T(8,128)(2,1)S(1)}, bf16[30,256]{1,0:T(8,128)(2,1)S(1)}, u32[]{:S(2)}, u32[]{:S(2)}) collective-permute-start(bf16[30,256]{1,0:T(8,128)(2,1)S(1)} %slice.281), channel_id=1, source_target_pairs={{0,4},{4,8},{8,12},{12,16},{16,20},{20,24},{24,28},{28,32},{32,36}... | collective-permute-start | bytes 46088 | tf_op jit(solution)/shard_map/ppermute | solution.py:13
  222.7 147.0 %all-to-all-start.1 = ((bf16[64,18,2048]{2,1,0:T(8,128)(2,1)}), bf16[64,18,2048]{2,1,0:T(8,128)(2,1)}, u32[]{:S(2)}, u32[]{:S(2)}) async-start(bf16[64,18,2048]{2,1,0:T(8,128)(2,1)} %reshape.114), calls=%async_computation.2 | async-start | bytes 12582912 | tf_op jit(solution)/shard_map/all_to_all | solution.py:79
  231.5 180.1 %reduce-scatter.2.cloned.1.call-start = ((), (), s32[]{:S(2)}) async-start(), calls=%async_computation.3 | async-start | bytes 5242880 | tf_op jit(solution)/shard_map/reduce_scatter | solution.py:40
  254.5 0.7 copy-start.4
  406.7 4.9 %copy-start.1 = (bf16[1,512,2048]{2,1,0:T(8,128)(2,1)S(1)}, bf16[1,512,2048]{2,1,0:T(8,128)(2,1)}, u32[]{:S(2)}) copy-start(bf16[1,512,2048]{2,1,0:T(8,128)(2,1)} %param.25) | copy-start | bytes 6291460
Sparse Core Ops, SparseCore 0:
  254.6 48.5 reduce-scatter.1
where the time goes:
time: 424 us; the launch traced here: 418 us
  waiting for transfers between devices  248 us (58%)
  local copies, waits for them, and re-layouts  83.2 us (20%)
  matrix products  22.7 us (5%)
  starting transfers between devices  22 us (5%)
  other arithmetic  17.3 us (4%)
  between operations  14.3 us (3%)
  blocking collectives  11.1 us (3%)
    all_to_all x1, waiting for transfers between devices, moe_half(): lax.all_to_all(send_buffer, 'ep', split_axis=0, concat_axis=0, tiled=True)  133 us
    all_to_all x1, waiting for transfers between devices, moe_half(): lax.all_to_all(result.reshape(arrived.shape), 'ep', split_axis=0, concat_...  115 us
    gather x1, local copies, waits for them, and re-layouts, moe_half(): padded_in[slot_token].reshape(experts_all, capacity, model_width)  12.3 us
    psum x1, blocking collectives, conv_half(): lax.psum((jnp.sum(filtered, axis=1), jnp.sum(filtered * filtered, axis=1)...  11.1 us
    all_to_all x1, starting transfers between devices, moe_half(): lax.all_to_all(send_buffer, 'ep', split_axis=0, concat_axis=0, tiled=True)  11 us
    dot_general x1, matrix products, moe_half(): jnp.dot(inner, expert_down[0], preferred_element_type=jnp.float32)  11 us
    gather x1, local copies, waits for them, and re-layouts, moe_half(): picked = returned_flat[slot_index].reshape(rows, TOP, model_width)  10 us
    all_to_all x1, starting transfers between devices, moe_half(): lax.all_to_all(result.reshape(arrived.shape), 'ep', split_axis=0, concat_...  8.72 us
  transfers between devices with their start and end apart: 4, of which 2 were waited for; matrix products, arithmetic and copies ran while one was open for 21% of the time, Pallas kernels for 0%

commit v1 on v0

v1 whole, which is shorter than its diff:
```python
import jax
import jax.numpy as jnp
from jax import lax
from jax.experimental import pallas as pl
from jax.experimental.pallas import tpu as pltpu
from jax.sharding import PartitionSpec as P

CONV = 1024
TOP = 2
MAIN = 16
EXTRA = 2
PIECE = 256
PIECES = 8
GROUP = 16


def passed_along(x, axis, by):
    peers = lax.axis_size(axis)
    pairs = [(i, i + by) for i in range(peers) if 0 <= i + by < peers]
    return lax.ppermute(x, axis, pairs)


def iota(shape, dimension):
    return lax.broadcasted_iota(jnp.int32, shape, dimension)


def fold_matrix():
    i = iota((PIECE, PIECE), 0)
    c = iota((PIECE, PIECE), 1)
    return (c == (i % PIECES) * (2 * GROUP) + i // PIECES).astype(jnp.bfloat16)


def unfold_matrix():
    i = iota((PIECE, PIECE), 1)
    c = iota((PIECE, PIECE), 0)
    return (c == (i % PIECES) * (2 * GROUP) + i // PIECES).astype(jnp.bfloat16)


def dot(a, b):
    return jnp.dot(a, b, preferred_element_type=jnp.float32)


def folded(rows):
    stacked = jnp.concatenate([rows[:, PIECE * k : PIECE * (k + 1)] for k in range(PIECES)], 0)
    return dot(fold_matrix(), stacked).astype(jnp.bfloat16)


def unfolded(block):
    stacked = dot(unfold_matrix(), block).astype(jnp.bfloat16)
    n = 2 * GROUP
    return jnp.concatenate([stacked[n * k : n * (k + 1)] for k in range(PIECES)], 1)


def send_kernel(route_ref, x_ref, gain_ref, send_ref, xn_ref, ids_ref):
    tokens, width = x_ref.shape
    experts = send_ref.shape[0]
    chunk = 32

    def norm(i, carry):
        rows = pl.ds(pl.multiple_of(i * chunk, chunk), chunk)
        x = x_ref[rows, :].astype(jnp.float32)
        scale = lax.rsqrt(jnp.mean(x * x, axis=-1, keepdims=True) + 1e-06)
        xn_ref[rows, :] = (x * scale * gain_ref[...]).astype(jnp.bfloat16)
        return carry

    lax.fori_loop(0, tokens // chunk, norm, 0)

    expert = iota((experts, tokens), 0)
    first, second = route_ref[0:1, :], route_ref[1:2, :]
    is_first, is_second = expert == first, expert == second
    hits = (is_first | is_second).astype(jnp.bfloat16)
    earlier = (iota((tokens, tokens), 0) < iota((tokens, tokens), 1)).astype(jnp.bfloat16)
    counts = dot(hits, earlier)
    for row, (mask, named) in enumerate(((is_first, first), (is_second, second))):
        rank = jnp.sum(jnp.where(mask, counts, 0.0), axis=0, keepdims=True).astype(jnp.int32)
        main = jnp.where(rank < MAIN, named * MAIN + rank, -1)
        extra = jnp.where((rank >= MAIN) & (rank < MAIN + EXTRA), named * EXTRA + rank - MAIN, -1)
        ids_ref[row : row + 1, :] = main
        ids_ref[row + 2 : row + 3, :] = extra

    def group(g, carry):
        row = iota((GROUP * MAIN, tokens), 0) + g * (GROUP * MAIN)
        pick = ((row == ids_ref[0:1, :]) | (row == ids_ref[1:2, :])).astype(jnp.bfloat16)
        low = iota((GROUP * EXTRA, tokens), 0) + g * (GROUP * EXTRA)
        more = ((low == ids_ref[2:3, :]) | (low == ids_ref[3:4, :])).astype(jnp.bfloat16)
        here = pl.ds(g * GROUP, GROUP)
        send_ref[here, :, 0:width] = (
            dot(pick, xn_ref[...]).astype(jnp.bfloat16).reshape(GROUP, MAIN, width)
        )
        rest = dot(more, xn_ref[...]).astype(jnp.bfloat16)
        send_ref[here, :, width:] = folded(rest).reshape(GROUP, MAIN, PIECE)
        return carry

    lax.fori_loop(0, experts // GROUP, group, 0)


def expert_kernel(in_ref, gate_ref, up_ref, down_ref, out_ref):
    width = gate_ref.shape[0]
    sources = in_ref.shape[0]
    both = 2

    def block(b, carry):
        parts = []
        for j in range(both):
            here = pl.ds((b * both + j) * GROUP, GROUP)
            parts.append(in_ref[here, :, 0:width].reshape(GROUP * MAIN, width))
        for j in range(both):
            here = pl.ds((b * both + j) * GROUP, GROUP)
            parts.append(unfolded(in_ref[here, :, width:].reshape(PIECE, PIECE)))
        rows = jnp.concatenate(parts, 0)
        gate = dot(rows, gate_ref[...])
        up = dot(rows, up_ref[...])
        inner = (gate / (1.0 + jnp.exp(-gate)) * up).astype(jnp.bfloat16)
        result = dot(inner, down_ref[...]).astype(jnp.bfloat16)
        for j in range(both):
            here = pl.ds((b * both + j) * GROUP, GROUP)
            top = j * GROUP * MAIN
            out_ref[here, :, 0:width] = result[top : top + GROUP * MAIN].reshape(GROUP, MAIN, width)
            low = both * GROUP * MAIN + j * GROUP * EXTRA
            out_ref[here, :, width:] = folded(result[low : low + GROUP * EXTRA]).reshape(
                GROUP, MAIN, PIECE
            )
        return carry

    lax.fori_loop(0, sources // (GROUP * both), block, 0)


def weight_kernel(route_ref, score_ref, main_ref, extra_ref):
    tokens = route_ref.shape[0]
    experts = main_ref.shape[1] // MAIN
    expert = iota((tokens, experts), 1)
    first, second = route_ref[:, 0:1], route_ref[:, 1:2]
    is_first, is_second = expert == first, expert == second
    hits = (is_first | is_second).astype(jnp.bfloat16)
    earlier = (iota((tokens, tokens), 0) > iota((tokens, tokens), 1)).astype(jnp.bfloat16)
    counts = dot(earlier, hits)
    group = jax.nn.sigmoid(score_ref[:, 0:1])
    pair = score_ref[:, 1:2]
    weights = (group * jax.nn.sigmoid(pair), group * jax.nn.sigmoid(-pair))
    places = []
    for mask, named in ((is_first, first), (is_second, second)):
        rank = jnp.sum(jnp.where(mask, counts, 0.0), axis=1, keepdims=True).astype(jnp.int32)
        places.append(
            (
                jnp.where(rank < MAIN, named * MAIN + rank, -1),
                jnp.where((rank >= MAIN) & (rank < MAIN + EXTRA), named * EXTRA + rank - MAIN, -1),
            )
        )
    for ref, which in ((main_ref, 0), (extra_ref, 1)):
        n = ref.shape[1]
        step = min(n, 256)
        for low in range(0, n, step):
            column = iota((tokens, step), 1) + low
            value = jnp.where(column == places[0][which], weights[0], 0.0)
            value = jnp.where(column == places[1][which], weights[1], value)
            high = value.astype(jnp.bfloat16)
            ref[0:tokens, low : low + step] = high
            ref[tokens:, low : low + step] = (value - high.astype(jnp.float32)).astype(jnp.bfloat16)


def combine_kernel(back_ref, main_ref, extra_ref, out_ref, rest_ref):
    experts, _, wide = back_ref.shape
    width = wide - PIECE
    tokens = out_ref.shape[0]
    for g in range(experts // GROUP):
        block = back_ref[g * GROUP : (g + 1) * GROUP, :, width:].reshape(PIECE, PIECE)
        rest_ref[g * 2 * GROUP : (g + 1) * 2 * GROUP, :] = unfolded(block)
    step = 256

    def columns(i, carry):
        here = pl.ds(pl.multiple_of(i * step, step), step)
        rows = back_ref[:, :, here].reshape(experts * MAIN, step)
        total = dot(main_ref[...], rows) + dot(extra_ref[...], rest_ref[:, here])
        out_ref[:, here] = (total[:tokens] + total[tokens:]).astype(jnp.bfloat16)
        return carry

    lax.fori_loop(0, width // step, columns, 0)


VMEM = pl.BlockSpec(memory_space=pltpu.VMEM)


def call(kernel, name, outs, scratch, limit, flops, nbytes, *args):
    return pl.pallas_call(
        kernel,
        name=name,
        out_shape=outs,
        in_specs=[VMEM] * len(args),
        out_specs=jax.tree.map(lambda _: VMEM, outs),
        scratch_shapes=scratch,
        compiler_params=pltpu.CompilerParams(vmem_limit_bytes=limit << 20),
        cost_estimate=pl.CostEstimate(flops=flops, bytes_accessed=nbytes, transcendentals=0),
    )(*args)


def conv_half(conv_value, conv_gate, depth_weight, norm_gain, norm_shift, conv_out_weight):
    channels = conv_value.shape[1]
    length = conv_value.shape[0]
    first_col = lax.axis_index("tp") * channels
    taps = lax.dynamic_slice_in_dim(depth_weight, first_col, channels, 1)
    gains = lax.dynamic_slice_in_dim(norm_gain, first_col, channels, 0)
    shifts = lax.dynamic_slice_in_dim(norm_shift, first_col, channels, 0)
    gated = (conv_value.astype(jnp.float32) * jax.nn.sigmoid(conv_gate.astype(jnp.float32))).astype(
        jnp.bfloat16
    )
    reach = taps.shape[0] - 1
    earlier = passed_along(gated[length - reach :], "ep", 1)
    padded = jnp.concatenate([earlier, gated], 0).astype(jnp.float32)
    filtered = taps[0] * padded[0:length]
    for offset in range(1, reach + 1):
        filtered = filtered + taps[offset] * padded[offset : offset + length]
    sums, squares = lax.psum(
        (jnp.sum(filtered, axis=1), jnp.sum(filtered * filtered, axis=1)), "tp"
    )
    center = (sums / CONV)[:, None]
    spread = (squares / CONV)[:, None] - center * center
    normed = (filtered - center) * lax.rsqrt(spread + 1e-05) * gains + shifts
    activated = jax.nn.silu(normed).astype(jnp.bfloat16)
    partial = jnp.dot(activated, conv_out_weight, preferred_element_type=jnp.float32).astype(
        jnp.bfloat16
    )
    peers = lax.axis_size("tp")
    me = lax.axis_index("tp")
    rows = length // peers
    total = lax.dynamic_slice_in_dim(partial, me * rows, rows, 0).astype(jnp.float32)
    for by in range(1, peers):
        theirs = lax.dynamic_slice_in_dim(partial, ((me + by) % peers) * rows, rows, 0)
        came = lax.ppermute(theirs, "tp", [(i, (i + by) % peers) for i in range(peers)])
        total = total + came.astype(jnp.float32)
    return total.astype(jnp.bfloat16)


def moe_half(moe_input, moe_gain, route_experts, route_scores, expert_gate, expert_up, expert_down):
    tokens, width = moe_input.shape
    experts = lax.axis_size("ep")
    hidden = expert_gate.shape[2]
    slots = experts * (MAIN + EXTRA)
    wide = jax.ShapeDtypeStruct((experts, MAIN, width + PIECE), jnp.bfloat16)
    send = call(
        send_kernel,
        "send",
        wide,
        [pltpu.VMEM((tokens, width), jnp.bfloat16), pltpu.VMEM((8, tokens), jnp.int32)],
        24,
        2 * slots * tokens * width,
        slots * width * 4,
        route_experts.T,
        moe_input,
        moe_gain[None, :],
    )
    arrived = lax.all_to_all(send, "ep", split_axis=0, concat_axis=0, tiled=True)
    main, extra = call(
        weight_kernel,
        "weights",
        (
            jax.ShapeDtypeStruct((2 * tokens, experts * MAIN), jnp.bfloat16),
            jax.ShapeDtypeStruct((2 * tokens, experts * EXTRA), jnp.bfloat16),
        ),
        [],
        16,
        2 * tokens * tokens * experts,
        4 * tokens * slots,
        route_experts,
        route_scores,
    )
    result = call(
        expert_kernel,
        "expert",
        wide,
        [],
        24,
        6 * slots * width * hidden,
        slots * width * 4,
        arrived,
        expert_gate[0],
        expert_up[0],
        expert_down[0],
    )
    returned = lax.all_to_all(result, "ep", split_axis=0, concat_axis=0, tiled=True)
    return call(
        combine_kernel,
        "combine",
        jax.ShapeDtypeStruct((tokens, width), jnp.bfloat16),
        [pltpu.VMEM((experts * EXTRA, width), jnp.bfloat16)],
        16,
        4 * slots * tokens * width,
        slots * width * 2,
        returned,
        main,
        extra,
    )


def on_device(
    conv_value,
    conv_gate,
    depth_weight,
    norm_gain,
    norm_shift,
    conv_out_weight,
    moe_input,
    moe_gain,
    route_experts,
    route_scores,
    expert_gate,
    expert_up,
    expert_down,
):
    conv_out = conv_half(
        conv_value, conv_gate, depth_weight, norm_gain, norm_shift, conv_out_weight
    )
    moe_out = moe_half(
        moe_input, moe_gain, route_experts, route_scores, expert_gate, expert_up, expert_down
    )
    return (conv_out, moe_out)


def solution(mesh):
    in_specs = (
        P("ep", "tp"),
        P("ep", "tp"),
        P(),
        P(),
        P(),
        P("tp", None),
        P(("ep", "tp"), None),
        P(),
        P(("ep", "tp"), None),
        P(("ep", "tp"), None),
        P("ep", None, None),
        P("ep", None, None),
        P("ep", None, None),
    )
    out_specs = (P(("ep", "tp"), None), P(("ep", "tp"), None))
    return jax.shard_map(
        on_device, mesh=mesh, in_specs=in_specs, out_specs=out_specs, check_vma=False
    )
```

time: 424 us -> 310 us (0.73); the launches traced: 418 us -> 310 us
  waiting for transfers between devices: 248 us -> 122 us
  blocking collectives: 11.1 us -> 129 us
  local copies, waits for them, and re-layouts: 83.2 us -> 12.5 us
  Pallas kernels: 0 us -> 25 us
  matrix products: 22.7 us -> 1.41 us
  between operations: 14.3 us -> 0.91 us
  starting transfers between devices: 22 us -> 10.9 us
  other arithmetic: 17.3 us -> 8.82 us
    all_to_all x2 -> x1, waiting for transfers between devices: 248 us -> 0.01 us  [moe_half(): lax.all_to_all(result, 'ep', split_axis=0, concat_axis=0, tiled=True)]
    all_to_all x0 -> x1, blocking collectives: none -> 118 us  [moe_half(): lax.all_to_all(send, 'ep', split_axis=0, concat_axis=0, tiled=True)]
    ppermute x1, waiting for transfers between devices: 0.01 us -> 97.7 us  [passed_along(): return lax.ppermute(x, axis, pairs)]
    reshape x5 -> x0, local copies, waits for them, and re-layouts: 36.7 us -> none  [the longest x1 7.77 us: moe_half(): flat_rows = arrived.reshape(-1, model_width)]
    pallas_call x0 -> x4, Pallas kernels: none -> 25 us  [call(): pl.pallas_call(kernel, name=name, out_shape=outs, in_specs=[VMEM] * len(a...]
    ppermute x0 -> x3, waiting for transfers between devices: none -> 24.1 us  [conv_half(): lax.ppermute(theirs, 'tp', [(i, (i + by) % peers) for i in range(peers)])]
    gather x2 -> x0, local copies, waits for them, and re-layouts: 22.3 us -> none  [the longest x1 12.3 us: moe_half(): padded_in[slot_token].reshape(experts_all, capacity, model_width)]
    dot_general x2 -> x0, matrix products: 18.1 us -> none  [the longest x1 11 us: moe_half(): jnp.dot(inner, expert_down[0], preferred_element_type=jnp.float32)]
  transfers between devices with their start and end apart: 4 -> 5, of which waited for: 2 -> 4; matrix products, arithmetic and copies ran while one was open for 21% -> 5% of each run, Pallas kernels for 0% -> 0%
where the time goes in v1:
time: 310 us
  blocking collectives  129 us (42%)
  waiting for transfers between devices  122 us (39%)
  Pallas kernels  25 us (8%)
  local copies, waits for them, and re-layouts  12.5 us (4%)
  starting transfers between devices  10.9 us (4%)
  other arithmetic  8.82 us (3%)
    all_to_all x1, blocking collectives, moe_half(): lax.all_to_all(send, 'ep', split_axis=0, concat_axis=0, tiled=True)  118 us
    ppermute x1, waiting for transfers between devices, passed_along(): return lax.ppermute(x, axis, pairs)  97.7 us
    pallas_call x4, Pallas kernels, call(): pl.pallas_call(kernel, name=name, out_shape=outs, in_specs=[VMEM] * len(a...  25 us
    ppermute x3, waiting for transfers between devices, conv_half(): lax.ppermute(theirs, 'tp', [(i, (i + by) % peers) for i in range(peers)])  24.1 us
    psum x1, blocking collectives, conv_half(): lax.psum((jnp.sum(filtered, axis=1), jnp.sum(filtered * filtered, axis=1)...  10.9 us
    unnamed x28, local copies, waits for them, and re-layouts  6.66 us
    all_to_all x1, starting transfers between devices, moe_half(): lax.all_to_all(result, 'ep', split_axis=0, concat_axis=0, tiled=True)  6.59 us
  transfers between devices with their start and end apart: 5, of which 4 were waited for; matrix products, arithmetic and copies ran while one was open for 5% of the time, Pallas kernels for 0%

profile of v1, /device:TPU:96, one launch (start us, length us, event | category | flops | bytes accessed | tf_op | source)
XLA Modules:
  0.0 309.9 jit_solution(17827166291067304303)
XLA Ops:
  0.7 0.8 copy-done.2
  1.4 1.4 copy-done.7
  3.5 6.5 %send.1 = bf16[64,16,2304]{2,1,0:T(8,128)(2,1)S(1)} custom-call(s32[2,384]{1,0:T(2,128)S(1)} %bitcast.37, bf16[384,2048]{1,0:T(8,128)(2,1)S(1)} %copy-done.7, f32[1,2048]{1,0:T(1,128)S(1)} %bitcast.41), custom_call_target="tpu_custom_call" | custom-call | flops 1811939328 | bytes 9437184 | tf_op jit(solution)/shard_map/send/pallas_call | solution.py:184
  10.0 117.8 %all_to_all.10.in_ref = bf16[64,16,2304]{2,1,0:T(8,128)(2,1)S(1)} all-to-all(bf16[64,16,2304]{2,1,0:T(8,128)(2,1)S(1)} %send.1), channel_id=1, replica_groups=mesh['ep'=64,'tp'=4] {'ep'}, dimensions={0} | all-to-all | bytes 9437184 | tf_op jit(solution)/shard_map/all_to_all | solution.py:251
  127.8 8.3 %expert.1 = bf16[64,16,2304]{2,1,0:T(8,128)(2,1)S(1)} custom-call(bf16[64,16,2304]{2,1,0:T(8,128)(2,1)S(1)} %all_to_all.10.in_ref, bf16[2048,512]{1,0:T(8,128)(2,1)S(1)} %bitcast.38, bf16[2048,512]{1,0:T(8,128)(2,1)S(1)} %bitcast.39, bf16[512,2048]{1,0:T(8,128)(2,1)S(1)} %bitcast.40), custom_call_target="tpu_custom_call" | custom-call | flops 7247757312 | bytes 9437184 | tf_op jit(solution)/shard_map/expert/pallas_call | solution.py:184
  136.1 2.2 copy-done.1
  138.2 6.6 %all-to-all-start.1 = ((bf16[64,16,2304]{2,1,0:T(8,128)(2,1)}), bf16[64,16,2304]{2,1,0:T(8,128)(2,1)}, u32[]{:S(2)}, u32[]{:S(2)}) async-start(bf16[64,16,2304]{2,1,0:T(8,128)(2,1)} %copy-done.1), calls=%async_computation.1 | async-start | bytes 9437184 | tf_op jit(solution)/shard_map/all_to_all | solution.py:279
  145.2 2.0 collective-permute-start
  147.2 1.4 constant_dynamic-slice_fusion
  148.6 1.2 fusion.38
  149.8 0.8 dynamic_slice.23
  151.4 97.7 %collective-permute-done = bf16[30,256]{1,0:T(8,128)(2,1)S(1)} collective-permute-done((bf16[30,256]{1,0:T(8,128)(2,1)S(1)}, bf16[30,256]{1,0:T(8,128)(2,1)S(1)}, u32[]{:S(2)}, u32[]{:S(2)}) %collective-permute-start) | collective-permute-done | bytes 15392 | tf_op jit(solution)/shard_map/ppermute | solution.py:20
  249.1 4.5 %fusion.36 = (f32[1024]{0:T(1024)S(1)}, f32[1024]{0:T(1024)S(1)}, f32[1024,256]{1,0:T(8,128)S(1)}) fusion(f32[1054,256]{1,0:T(8,128)S(1)} %maximum_convert_fusion, f32[256]{0:T(256)S(1)} %bitcast.72, f32[256]{0:T(256)S(1)} %bitcast.43, f32[256]{0:T(256)S(1)} %bitcast.44, f32[256]{0:T(256)S(1)} %bitcast.45, f32[256]{0:T(256)S(1)} %bitcast.46, ...), kind=kLoop, calls=%fused_computation.79 | loop fusion | flops 16775168 | bytes 33594368 | tf_op jit(solution)/shard_map/reduce_sum | solution.py:213
  253.7 10.9 %all-reduce = (f32[1024]{0:T(1024)S(1)}, f32[1024]{0:T(1024)S(1)}) all-reduce(f32[1024]{0:T(1024)S(1)} %get-tuple-element.7, f32[1024]{0:T(1024)S(1)} %get-tuple-element.6), channel_id=1, replica_groups=mesh['ep'=64,'tp'=4] {'tp'}, use_global_device_ids=true, to_apply=%region_3.0 | all-reduce | flops 2048 | bytes 16384 | tf_op jit(solution)/shard_map/psum | solution.py:212
  264.5 1.4 convolution_convert_fusion
  266.0 1.7 constant_dynamic-slice_fusion.3
  267.7 1.3 copy-done.9
  269.0 1.6 collective-permute-start.2
  271.6 1.2 weights.1
  272.8 11.3 %collective-permute-done.3 = bf16[256,2048]{1,0:T(8,128)(2,1)} collective-permute-done((bf16[256,2048]{1,0:T(8,128)(2,1)}, bf16[256,2048]{1,0:T(8,128)(2,1)}, u32[]{:S(2)}, u32[]{:S(2)}) %collective-permute-start.3) | collective-permute-done | bytes 1048608 | tf_op jit(solution)/shard_map/ppermute | solution.py:228
  284.1 1.6 collective-permute-done.2
  285.7 11.1 %collective-permute-done.1 = bf16[256,2048]{1,0:T(8,128)(2,1)} collective-permute-done((bf16[256,2048]{1,0:T(8,128)(2,1)}, bf16[256,2048]{1,0:T(8,128)(2,1)}, u32[]{:S(2)}, u32[]{:S(2)}) %collective-permute-start.1) | collective-permute-done | bytes 1048608 | tf_op jit(solution)/shard_map/ppermute | solution.py:228
  296.9 3.9 %add_convert_fusion = bf16[256,2048]{1,0:T(8,128)(2,1)} fusion(bf16[256,2048]{1,0:T(8,128)(2,1)} %collective-permute-done.3, bf16[256,2048]{1,0:T(8,128)(2,1)} %collective-permute-done.2, bf16[256,2048]{1,0:T(8,128)(2,1)} %collective-permute-done.1, bf16[1024,2048]{1,0:T(8,128)(2,1)} %copy-done.9, s32[]{:T(128)S(6)} %select_n.30), kind=kLoop, calls=%fused_computation.1 | loop fusion | flops 4194304 | bytes 5242884 | tf_op jit(solution)/shard_map/convert_element_type | solution.py:230
  300.8 9.1 %combine.1 = bf16[384,2048]{1,0:T(8,128)(2,1)} custom-call(bf16[64,16,2304]{2,1,0:T(8,128)(2,1)} %all-to-all-done.1.back_ref, bf16[768,1024]{1,0:T(8,128)(2,1)S(1)} %get-tuple-element.4.main_ref, bf16[768,128]{1,0:T(8,128)(2,1)S(1)} %get-tuple-element.5.extra_ref), custom_call_target="tpu_custom_call" | custom-call | flops 3623878656 | bytes 4718592 | tf_op jit(solution)/shard_map/combine/pallas_call | solution.py:184
  (32 shorter events, 2.9 us)
Async XLA Ops:
  0.6 263.9 %copy-start = (bf16[256,2048]{1,0:T(8,128)(2,1)S(1)}, bf16[256,2048]{1,0:T(8,128)(2,1)}, u32[]{:S(2)}) copy-start(bf16[256,2048]{1,0:T(8,128)(2,1)} %param.18) | copy-start | bytes 3145732
  0.6 0.8 copy-start.2
  1.4 1.4 copy-start.7
  2.8 0.7 copy-start.8
  10.0 117.8 %copy-start.4 = (bf16[1,2048,512]{2,1,0:T(8,128)(2,1)S(1)}, bf16[1,2048,512]{2,1,0:T(8,128)(2,1)}, u32[]{:S(2)}) copy-start(bf16[1,2048,512]{2,1,0:T(8,128)(2,1)} %param.23) | copy-start | bytes 6291460
  10.0 117.8 %copy-start.5 = (bf16[1,2048,512]{2,1,0:T(8,128)(2,1)S(1)}, bf16[1,2048,512]{2,1,0:T(8,128)(2,1)}, u32[]{:S(2)}) copy-start(bf16[1,2048,512]{2,1,0:T(8,128)(2,1)} %param.24) | copy-start | bytes 6291460
  10.0 117.8 %copy-start.6 = (bf16[1,512,2048]{2,1,0:T(8,128)(2,1)S(1)}, bf16[1,512,2048]{2,1,0:T(8,128)(2,1)}, u32[]{:S(2)}) copy-start(bf16[1,512,2048]{2,1,0:T(8,128)(2,1)} %param.25) | copy-start | bytes 6291460
  136.1 2.2 copy-start.1
  138.2 6.6 %copy-start.10 = (bf16[1024,256]{1,0:T(8,128)(2,1)S(1)}, bf16[1024,256]{1,0:T(8,128)(2,1)}, u32[]{:S(2)}) copy-start(bf16[1024,256]{1,0:T(8,128)(2,1)} %param.14) | copy-start | bytes 1572868
  138.2 6.6 %copy-start.11 = (bf16[1024,256]{1,0:T(8,128)(2,1)S(1)}, bf16[1024,256]{1,0:T(8,128)(2,1)}, u32[]{:S(2)}) copy-start(bf16[1024,256]{1,0:T(8,128)(2,1)} %param.13) | copy-start | bytes 1572868
  138.2 162.5 %all-to-all-start.1 = ((bf16[64,16,2304]{2,1,0:T(8,128)(2,1)}), bf16[64,16,2304]{2,1,0:T(8,128)(2,1)}, u32[]{:S(2)}, u32[]{:S(2)}) async-start(bf16[64,16,2304]{2,1,0:T(8,128)(2,1)} %copy-done.1), calls=%async_computation.1 | async-start | bytes 9437184 | tf_op jit(solution)/shard_map/all_to_all | solution.py:279
  145.2 103.9 %collective-permute-start = (bf16[30,256]{1,0:T(8,128)(2,1)S(1)}, bf16[30,256]{1,0:T(8,128)(2,1)S(1)}, u32[]{:S(2)}, u32[]{:S(2)}) collective-permute-start(bf16[30,256]{1,0:T(8,128)(2,1)S(1)} %slice.252), channel_id=1, source_target_pairs={{0,4},{4,8},{8,12},{12,16},{16,20},{20,24},{24,28},{28,32},{32,36}... | collective-permute-start | bytes 46088 | tf_op jit(solution)/shard_map/ppermute | solution.py:20
  266.0 3.0 copy-start.9
  266.0 5.3 %copy-start.3 = (s32[384,2]{0,1:T(2,128)S(1)}, s32[384,2]{0,1:T(2,128)}, u32[]{:S(2)}) copy-start(s32[384,2]{0,1:T(2,128)} %param.21) | copy-start | bytes 9220
  266.0 5.4 %copy-start.12 = (f32[384,2]{0,1:T(2,128)S(1)}, f32[384,2]{0,1:T(2,128)}, u32[]{:S(2)}) copy-start(f32[384,2]{0,1:T(2,128)} %param.22) | copy-start | bytes 9220
  269.0 15.1 %collective-permute-start.3 = (bf16[256,2048]{1,0:T(8,128)(2,1)}, bf16[256,2048]{1,0:T(8,128)(2,1)}, u32[]{:S(2)}, u32[]{:S(2)}) collective-permute-start(bf16[256,2048]{1,0:T(8,128)(2,1)} %get-tuple-element.12), channel_id=1, source_target_pairs={{0,3},{1,0},{2,1},{3,2},{4,7},{5,4},{6,5},{7,6},{8,11},{9,8},{10,9... | collective-permute-start | bytes 3145736 | tf_op jit(solution)/shard_map/ppermute | solution.py:228
  269.0 16.7 %collective-permute-start.2 = (bf16[256,2048]{1,0:T(8,128)(2,1)}, bf16[256,2048]{1,0:T(8,128)(2,1)}, u32[]{:S(2)}, u32[]{:S(2)}) collective-permute-start(bf16[256,2048]{1,0:T(8,128)(2,1)} %get-tuple-element.13), channel_id=1, source_target_pairs={{0,2},{1,3},{2,0},{3,1},{4,6},{5,7},{6,4},{7,5},{8,10},{9,11},{10,... | collective-permute-start | bytes 3145736 | tf_op jit(solution)/shard_map/ppermute | solution.py:228
  270.6 26.3 %collective-permute-start.1 = (bf16[256,2048]{1,0:T(8,128)(2,1)}, bf16[256,2048]{1,0:T(8,128)(2,1)}, u32[]{:S(2)}, u32[]{:S(2)}) collective-permute-start(bf16[256,2048]{1,0:T(8,128)(2,1)} %get-tuple-element.11), channel_id=1, source_target_pairs={{0,1},{1,2},{2,3},{3,0},{4,5},{5,6},{6,7},{7,4},{8,9},{9,10},{10,1... | collective-permute-start | bytes 3145736 | tf_op jit(solution)/shard_map/ppermute | solution.py:228
